TPU v7x, 32 devices: a whole 2x2x4 slice. The times are simulated.
32 devices in a mesh: sp: 8 (over z, y), tp: 4 (over x, core).
Axes of the slice: x: 2, y: 2, z: 4, core: 2. Of those that a mesh axis runs over, the one named last changes fastest.
Arguments:
- residual: bfloat16 [2048, 2048], P('sp'), may hold values from -6 to 6
- ssm_input: bfloat16 [2048, 1024], P('sp', 'tp'), may hold values from -6 to 6
- in_map: bfloat16 [2, 64, 16, 128], P(None, 'tp'), may hold values from -1 to 1
- out_map: bfloat16 [2, 64, 16, 128], P(None, 'tp'), may hold values from -0.5 to 0.5
- damping: float32 [64, 64], P('tp'), may hold values from 0.0001 to 0.24
- log_step: float32 [64], P('tp'), may hold values from -8 to -1.2
- frequency: float32 [64, 64], P('tp'), may hold values from 1 to 201.06177
- pacing: float32 [2048], P('sp'), may hold values from 0.28 to 3.5
- feedthrough: float32 [1024], P('tp'), may hold values from -4 to 4
- w_out: bfloat16 [1024, 2048], P('tp'), may hold values from -0.375 to 0.375
- gain_mix: float32 [2048], replicated, may hold values from 0.1 to 1.9
- w_gate: bfloat16 [2048, 5632], P('sp', 'tp'), may hold values from -0.125 to 0.125
- w_value: bfloat16 [2048, 5632], P('sp', 'tp'), may hold values from -0.125 to 0.125
- conv_taps: float32 [3, 5632], P(None, 'tp'), may hold values from -3 to 3
- w_down: bfloat16 [5632, 2048], P('tp', 'sp'), may hold values from -0.21875 to 0.21875
- gain_ffn: float32 [2048], replicated, may hold values from 0.1 to 1.9
Outputs:
- result: bfloat16 [2048, 2048], P(('sp', 'tp'))
All inputs are finite; a program needn't handle non-finite values.
Results may differ from a plain program's by a relative error of at most 0.02.
Values may be sent and summed in bfloat16 or wider, within the bound.
A program may use at most 128 MiB of HBM per device.

v0:
```python
import math
import jax
import jax.numpy as jnp
from jax import lax
from jax.sharding import PartitionSpec as P

deep_alpha = 8.0**0.25
norm_eps = 1e-06
highest = lax.Precision.HIGHEST


def carried_in(value, axis, join, neutral, backward):
    count, mine = (lax.axis_size(axis), lax.axis_index(axis))
    pieces = jax.tree.map(lambda part: lax.all_gather(part, axis), value)
    if backward:
        pieces = jax.tree.map(lambda part: part[::-1], pieces)
        mine = count - 1 - mine
    total = jax.tree.map(
        lambda part, zero: jnp.full_like(part, 0) + jnp.asarray(zero, part.dtype), value, neutral
    )

    def hop(position, total):
        longer = join(total, jax.tree.map(lambda part: part[position], pieces))
        return jax.tree.map(lambda new, old: jnp.where(position < mine, new, old), longer, total)

    return lax.fori_loop(0, count - 1, hop, total)


def extended(cells, sides, width):
    for axis, dim in sides:
        count = lax.axis_size(axis)
        ends = count - 1
        head = lax.slice_in_dim(cells, 0, width, axis=dim)
        tail = lax.slice_in_dim(cells, cells.shape[dim] - width, cells.shape[dim], axis=dim)
        cells = jnp.concatenate(
            [
                lax.ppermute(tail, axis, [(i, (i + 1) % count) for i in range(ends)]),
                cells,
                lax.ppermute(head, axis, [((i + 1) % count, i) for i in range(ends)]),
            ],
            axis=dim,
        )
    return cells


def normalize(pre_norm, gain_row):
    mean_row = jnp.mean(pre_norm, axis=-1, keepdims=True)
    centred = pre_norm - mean_row
    spread = jnp.mean(centred * centred, axis=-1, keepdims=True)
    return centred * lax.rsqrt(spread + norm_eps) * gain_row


def complex_mul(first_pair, second_pair):
    state_half = first_pair.shape[-1] // 2
    a_re = first_pair[..., :state_half]
    a_im = first_pair[..., state_half:]
    b_re = second_pair[..., :state_half]
    b_im = second_pair[..., state_half:]
    return jnp.concatenate([a_re * b_re - a_im * b_im, a_re * b_im + a_im * b_re], axis=-1)


def combine_pair(earlier, later):
    return (complex_mul(earlier[0], later[0]), complex_mul(later[0], earlier[1]) + later[1])


def unit_pair(groups, state_half):
    return jnp.concatenate(
        [jnp.ones((groups, state_half), jnp.float32), jnp.zeros((groups, state_half), jnp.float32)],
        axis=-1,
    )


def local_pass(u_rows, pace_rows, in_map_d, pair_re, pair_im, rate_inv, phase_shift):
    positions = u_rows.shape[0]
    groups = u_rows.shape[1]
    state_pair = pair_re.shape[1]
    block_len = min(64, positions)
    blocks = positions // block_len
    identity_pair = unit_pair(groups, state_pair // 2)
    inflow = jnp.einsum("tgc,gcq->tgq", u_rows, in_map_d, preferred_element_type=jnp.float32)
    deltas = pace_rows[:, None, None]
    decays = jnp.exp(pair_re * deltas) * jnp.cos(pair_im * deltas - phase_shift)
    driven = complex_mul(complex_mul(decays - identity_pair, rate_inv), inflow)
    within = jnp.cumsum(pace_rows.reshape(blocks, block_len), axis=1)[:, :, None, None]
    advance = jnp.exp(pair_re * within) * jnp.cos(pair_im * within - phase_shift)
    inverse = jnp.exp(-pair_re * within) * jnp.cos(pair_im * within + phase_shift)
    weighted = complex_mul(inverse, driven.reshape(blocks, block_len, groups, state_pair))
    triangle = (
        lax.broadcasted_iota(jnp.int32, (block_len, block_len), 0)
        >= lax.broadcasted_iota(jnp.int32, (block_len, block_len), 1)
    ).astype(jnp.float32)
    running = jnp.einsum(
        "st,btq->bsq",
        triangle,
        weighted.reshape(blocks, block_len, groups * state_pair),
        precision=highest,
    )
    running = running.reshape(blocks, block_len, groups, state_pair)

    def carry_step(state_now, block_terms):
        level_now, product_now = state_now
        total_now, end_now = block_terms
        return (
            (complex_mul(end_now, level_now + total_now), complex_mul(end_now, product_now)),
            (level_now, product_now),
        )

    start_pair = (jnp.zeros_like(identity_pair), identity_pair)
    last_pair, outputs = lax.scan(carry_step, start_pair, (running[:, -1], advance[:, -1]))
    return (advance, running, outputs[0], outputs[1], last_pair[1], last_pair[0])


def finish(pass_out, incoming, out_map_d):
    advance = pass_out[0]
    running = pass_out[1]
    starts = pass_out[2] + complex_mul(pass_out[3], incoming[None])
    states = complex_mul(advance, starts[:, None] + running)
    readout = jnp.einsum("bsgq,gcq->bsgc", states, out_map_d.astype(jnp.float32), precision=highest)
    return readout.reshape(readout.shape[0] * readout.shape[1], readout.shape[2], readout.shape[3])


def shards(
    residual,
    ssm_input,
    in_map,
    out_map,
    damping,
    log_step,
    frequency,
    pacing,
    feedthrough,
    w_out,
    gain_mix,
    w_gate,
    w_value,
    conv_taps,
    w_down,
    gain_ffn,
):
    positions = ssm_input.shape[0]
    channel_count = ssm_input.shape[1]
    groups = damping.shape[0]
    state_half = damping.shape[1]
    group_width = channel_count // groups
    own_rows = positions // lax.axis_size("tp")
    phase_shift = jnp.concatenate(
        [jnp.zeros((state_half,), jnp.float32), jnp.full((state_half,), 0.5 * math.pi, jnp.float32)]
    )
    rate_re = -damping
    step_col = jnp.exp(log_step)[:, None]
    pair_re = jnp.concatenate([rate_re, rate_re], axis=-1) * step_col
    pair_im = jnp.concatenate([frequency, frequency], axis=-1) * step_col
    modulus = rate_re * rate_re + frequency * frequency
    rate_inv = jnp.concatenate([rate_re / modulus, -frequency / modulus], axis=-1)
    u_rows = ssm_input.reshape(positions, groups, group_width)
    forward_pass = local_pass(u_rows, pacing, in_map[0], pair_re, pair_im, rate_inv, phase_shift)
    backward_pass = local_pass(
        u_rows[::-1], pacing[::-1], in_map[1], pair_re, pair_im, rate_inv, phase_shift
    )
    identity = (unit_pair(groups, state_half), jnp.zeros((groups, 2 * state_half), jnp.float32))
    forward_in = carried_in((forward_pass[4], forward_pass[5]), "sp", combine_pair, identity, False)
    backward_in = carried_in(
        (backward_pass[4], backward_pass[5]), "sp", combine_pair, identity, True
    )
    readout = (
        finish(forward_pass, forward_in[1], out_map[0])
        + finish(backward_pass, backward_in[1], out_map[1])[::-1]
    )
    readout = readout.reshape(positions, channel_count) + feedthrough * ssm_input.astype(
        jnp.float32
    )
    channels = jax.nn.gelu(readout).astype(jnp.bfloat16)
    mixed = lax.psum(
        jnp.dot(channels, w_out, preferred_element_type=jnp.float32).astype(jnp.bfloat16), "tp"
    ).astype(jnp.float32)
    whole_rows = normalize(deep_alpha * residual.astype(jnp.float32) + mixed, gain_mix).astype(
        jnp.bfloat16
    )
    norm_first = lax.dynamic_slice_in_dim(whole_rows, lax.axis_index("tp") * own_rows, own_rows, 0)
    first_kept = lax.optimization_barrier(norm_first).astype(jnp.float32)
    gate_sum = jnp.dot(
        whole_rows,
        lax.all_gather(w_gate, "sp", axis=0, tiled=True),
        preferred_element_type=jnp.float32,
    )
    value_sum = jnp.dot(
        whole_rows,
        lax.all_gather(w_value, "sp", axis=0, tiled=True),
        preferred_element_type=jnp.float32,
    )
    gated = gate_sum.astype(jnp.bfloat16)
    values = lax.optimization_barrier(value_sum.astype(jnp.bfloat16)).astype(jnp.float32)
    padded = extended(gated, (("sp", 0),), 1).astype(jnp.float32)
    smoothed = conv_taps[0] * padded[:-2] + conv_taps[1] * padded[1:-1] + conv_taps[2] * padded[2:]
    hidden = (jax.nn.gelu(smoothed) * values).astype(jnp.bfloat16)
    partials = jnp.dot(
        hidden, lax.all_gather(w_down, "sp", axis=1, tiled=True), preferred_element_type=jnp.float32
    )
    branch = lax.psum_scatter(
        partials.astype(jnp.bfloat16), "tp", scatter_dimension=0, tiled=True
    ).astype(jnp.float32)
    return normalize(deep_alpha * first_kept + branch, gain_ffn).astype(jnp.bfloat16)


def solution(mesh):
    in_specs = (
        P("sp", None),
        P("sp", "tp"),
        P(None, "tp", None, None),
        P(None, "tp", None, None),
        P("tp", None),
        P("tp"),
        P("tp", None),
        P("sp"),
        P("tp"),
        P("tp", None),
        P(),
        P("sp", "tp"),
        P("sp", "tp"),
        P(None, "tp"),
        P("tp", "sp"),
        P(),
    )
    out_specs = P(("sp", "tp"), None)
    return jax.shard_map(shards, mesh=mesh, in_specs=in_specs, out_specs=out_specs, check_vma=False)
```

profile of v0, /device:TPU:0, one launch (start us, length us, event | category | flops | bytes accessed | tf_op | source)
XLA Modules:
  0.0 552.3 jit_solution(3094445604148882098)
XLA Ops:
  7.4 0.9 rev.15
  8.2 0.8 reduce_window_sum.21
  9.0 0.7 copy.124
  9.7 0.7 exp.21
  10.4 1.0 copy.31
  11.4 0.3 rev.16
  11.7 1.4 convolution_bitcast_fusion.1
  13.1 1.8 convolution_bitcast_fusion
  15.2 14.3 %multiply_add_fusion.12 = (f32[256,16,128]{0,2,1:T(8,128)S(1)}, f32[256,16,128]{0,2,1:T(8,128)S(1)}) fusion(f32[256]{0:T(256)S(1)} %rev.15, f32[16,128]{1,0:T(8,128)S(1)} %copy-done.23, f32[128]{0:T(128)S(1)} %copy-done.25, f32[16,128]{1,0:T(8,128)S(1)} %get-tuple-element.459, f32[16,128]{1,0:T(8,128)S(1)} %get-tuple-element.399, f32[256]{0:T(256)S(1)} %copy-done.20), kind=kLoop, calls=%fused_computation.76 | loop fusion | flops 5242880 | bytes 4221440 | tf_op jit(solution)/shard_map/sub | solution.py:83
  29.5 1.1 multiply_subtract_fusion.10
  30.6 1.6 pad_maximum_fusion.4
  32.2 1.9 copy.54
  34.1 0.2 reduce_window_sum.24
  34.4 0.2 reduce_window_sum.22
  34.6 29.3 %fusion.9 = (f32[4,64,16,128]{3,1,0,2:T(8,128)S(1)}, f32[4,64,16,128]{3,1,0,2:T(8,128)}, f32[4,64,16,128]{3,1,0,2:T(8,128)S(1)}, f32[4,64,16,128]{3,1,0,2:T(8,128)S(1)}) fusion(f32[4,64]{1,0:T(4,128)S(1)} %reduce_window_sum.24, f32[128]{0:T(128)S(1)} %copy-done.27, f32[16,128]{1,0:T(8,128)S(1)} %get-tuple-element.398, f32[16,128]{1,0:T(8,128)S(1)} %get-tuple-element.459, ...), kind=kLoop, calls=%fused_computation.48 | loop fusion | flops 7340032 | bytes 8416256 | tf_op jit(solution)/shard_map/mul | solution.py:86
  64.0 1.6 multiply_subtract_fusion.7
  65.6 1.6 fusion.10
  67.2 0.4 copy.64
  67.6 1.0 copy-done.4
  68.7 0.8 while.61
  69.5 32.3 %all-gather.2 = f32[128,128]{1,0:T(8,128)S(1)} all-gather(f32[16,128]{1,0:T(8,128)S(1)} %get-tuple-element.280), channel_id=4, replica_groups=mesh['sp'=8,'tp'=4] {'sp'}, dimensions={0}, use_global_device_ids=true | all-gather | bytes 73728 | tf_op jit(solution)/shard_map/all_gather | solution.py:14
  101.8 30.5 %all-gather.3 = f32[128,128]{1,0:T(8,128)S(1)} all-gather(f32[16,128]{1,0:T(8,128)S(1)} %get-tuple-element.281), channel_id=5, replica_groups=mesh['sp'=8,'tp'=4] {'sp'}, dimensions={0}, use_global_device_ids=true | all-gather | bytes 73728 | tf_op jit(solution)/shard_map/all_gather | solution.py:14
  132.4 1.4 while.63
  133.9 0.8 maximum_add_fusion.3
  134.8 2.0 bitcast_add_fusion.2
  137.0 1.6 multiply_subtract_fusion.6
  138.6 2.7 fusion.36
  141.3 1.0 copy.48
  142.3 2.1 reshape.197
  144.3 1.8 rev.19
  146.1 2.9 copy.52
  149.1 4.6 multiply_subtract_fusion.9
  153.7 1.6 fusion.13
  155.3 0.4 copy.63
  155.7 0.9 copy-done.5
  156.8 0.8 while.60
  157.5 30.5 %all-gather = f32[128,128]{1,0:T(8,128)S(1)} all-gather(f32[16,128]{1,0:T(8,128)S(1)} %get-tuple-element.275), channel_id=2, replica_groups=mesh['sp'=8,'tp'=4] {'sp'}, dimensions={0}, use_global_device_ids=true | all-gather | bytes 73728 | tf_op jit(solution)/shard_map/all_gather | solution.py:14
  188.0 30.5 %all-gather.1 = f32[128,128]{1,0:T(8,128)S(1)} all-gather(f32[16,128]{1,0:T(8,128)S(1)} %get-tuple-element.276), channel_id=3, replica_groups=mesh['sp'=8,'tp'=4] {'sp'}, dimensions={0}, use_global_device_ids=true | all-gather | bytes 73728 | tf_op jit(solution)/shard_map/all_gather | solution.py:14
  218.6 1.4 while.62
  220.3 1.9 bitcast_add_fusion.3
  222.2 1.3 multiply_subtract_fusion.8
  223.5 2.7 fusion.39
  226.4 0.3 reshape.193
  227.1 1.4 convolution_convert_fusion.2
  228.6 0.5 all-gather.8.cloned.1.call-update
  229.2 0.5 all-gather.10.cloned.1.call-update
  229.7 0.5 all-gather.12.cloned.1.call-update
  230.4 35.7 %all-reduce.2.cloned.1.call-done = bf16[256,2048]{1,0:T(8,128)(2,1)} async-done(((bf16[256,2048]{1,0:T(8,128)(2,1)}), bf16[256,2048]{1,0:T(8,128)(2,1)}) %all-reduce.2.cloned.1.call-update) | async-done | bytes 1048592 | tf_op jit(solution)/shard_map/psum | solution.py:173
  266.1 1.7 fusion.24
  267.9 0.6 multiply_reduce_fusion
  268.4 1.6 multiply_convert_fusion
  270.0 54.2 %all-gather.8.cloned.1.call-done = bf16[2048,1408]{1,0:T(8,128)(2,1)} async-done(((bf16[256,1408]{1,0:T(8,128)(2,1)}), bf16[2048,1408]{1,0:T(8,128)(2,1)}) %all-gather.8.cloned.1.call-update) | async-done | bytes 5767184 | tf_op jit(solution)/shard_map/all_gather | solution.py:183
  324.2 4.8 convolution_convert_fusion.1
  329.0 2.5 collective-permute-start
  331.5 1.3 collective-permute-start.1
  332.8 83.8 %all-gather.10.cloned.1.call-done = bf16[2048,1408]{1,0:T(8,128)(2,1)} async-done(((bf16[256,1408]{1,0:T(8,128)(2,1)}), bf16[2048,1408]{1,0:T(8,128)(2,1)}) %all-gather.10.cloned.1.call-update) | async-done | bytes 5767184 | tf_op jit(solution)/shard_map/all_gather | solution.py:188
  416.6 5.3 convolution_convert_fusion
  421.9 1.3 maximum_convert_fusion
  423.2 86.4 %all-gather.12.cloned.1.call-done = bf16[1408,2048]{1,0:T(8,128)(2,1)} async-done(((bf16[1408,256]{1,0:T(8,128)(2,1)}), bf16[1408,2048]{1,0:T(8,128)(2,1)}) %all-gather.12.cloned.1.call-update) | async-done | bytes 5767184 | tf_op jit(solution)/shard_map/all_gather | solution.py:197
  509.6 7.7 %convolution_convert_fusion.3 = bf16[256,2048]{1,0:T(8,128)(2,1)} fusion(bf16[1408,2048]{1,0:T(8,128)(2,1)} %all-gather.12.cloned.1.call-done, f32[258,1408]{1,0:T(8,128)} %maximum_convert_fusion, bf16[256,1408]{1,0:T(8,128)(2,1)} %convolution_convert_fusion, f32[1408]{0:T(1024)S(1)} %get-tuple-element.348, f32[1408]{0:T(1024)S(1)} %get-tuple-element.349, ...), kind=kOutput, calls=%fused_computation.39 | convolution fusion | flops 1482686464 | bytes 11878912 | tf_op jit(solution)/shard_map/dot_general | solution.py:196
  517.3 23.1 %reduce-scatter.2.cloned.1.call-done = bf16[64,2048]{1,0:T(8,128)(2,1)} async-done(((bf16[256,2048]{1,0:T(8,128)(2,1)}), bf16[64,2048]{1,0:T(8,128)(2,1)}) %reduce-scatter.2.cloned.1.call-update) | async-done | bytes 262160 | tf_op jit(solution)/shard_map/reduce_scatter | solution.py:199
  540.4 1.1 fusion.50
  541.5 1.2 multiply_reduce_fusion.1
  542.7 1.8 multiply_convert_fusion.1
  (193 shorter events, 5.5 us)
Async XLA Ops:
  7.4 219.7 %copy-start = (bf16[256,2048]{1,0:T(8,128)(2,1)S(1)}, bf16[256,2048]{1,0:T(8,128)(2,1)}, u32[]{:S(2)}) copy-start(bf16[256,2048]{1,0:T(8,128)(2,1)} %param.33) | copy-start | bytes 3145732
  7.4 258.7 %all-reduce.2.cloned.1.call-start = ((), (), s32[]{:S(2)}) async-start(), calls=%async_computation.1 | async-start | bytes 2097152 | tf_op jit(solution)/shard_map/psum | solution.py:173
  9.7 5.3 copy-start.9
  11.6 1.5 copy-start.16
  11.7 3.4 copy-start.18
  11.7 3.4 copy-start.24
  11.7 3.5 copy-start.20
  11.7 3.5 copy-start.23
  11.7 3.4 copy-start.25
  15.2 14.3 %copy-start.8 = (f32[256,16,128]{0,2,1:T(8,128)S(1)}, f32[256,16,128]{0,2,1:T(8,128)}, u32[]{:S(2)}) copy-start(f32[256,16,128]{0,2,1:T(8,128)} %convolution_bitcast_fusion) | copy-start | bytes 6291460
  32.2 2.4 copy-start.27
  34.6 29.3 %copy-start.3 = (f32[256,16,128]{2,0,1:T(8,128)S(1)}, f32[256,16,128]{2,0,1:T(8,128)}, u32[]{:S(2)}) copy-start(f32[256,16,128]{2,0,1:T(8,128)} %copy.54) | copy-start | bytes 6291460
  64.0 4.7 copy-start.1
  67.2 1.4 copy-start.4
  67.2 1.5 copy-start.11
  69.5 32.3 %copy-start.17 = (f32[4,16,128]{2,1,0:T(8,128)}, f32[4,16,128]{2,1,0:T(8,128)S(1)}, u32[]{:S(2)}) copy-start(f32[4,16,128]{2,1,0:T(8,128)S(1)} %get-tuple-element.278) | copy-start | bytes 98308
  134.8 2.2 copy-start.2
  137.0 1.6 copy-start.14
  155.3 1.4 copy-start.5
  155.3 1.4 copy-start.10
  222.2 1.3 copy-start.15
  223.5 3.2 copy-start.13
  226.2 0.7 copy-start.26
  228.5 1.8 copy-start.19
  228.5 37.6 %copy-start.6 = (bf16[256,2048]{1,0:T(8,128)(2,1)S(1)}, bf16[256,2048]{1,0:T(8,128)(2,1)}, u32[]{:S(2)}) copy-start(bf16[256,2048]{1,0:T(8,128)(2,1)} %param.24) | copy-start | bytes 3145732
  228.5 95.7 %all-gather.8.cloned.1.call-start = ((), (), s32[]{:S(2)}) async-start(), calls=%async_computation.2 | async-start | bytes 6488064 | tf_op jit(solution)/shard_map/all_gather | solution.py:183
  229.1 187.5 %all-gather.10.cloned.1.call-start = ((), (), s32[]{:S(2)}) async-start(), calls=%async_computation.3 | async-start | bytes 6488064 | tf_op jit(solution)/shard_map/all_gather | solution.py:188
  229.7 279.9 %all-gather.12.cloned.1.call-start = ((), (), s32[]{:S(2)}) async-start(), calls=%async_computation.4 | async-start | bytes 6488064 | tf_op jit(solution)/shard_map/all_gather | solution.py:197
  230.3 310.1 %reduce-scatter.2.cloned.1.call-start = ((), (), s32[]{:S(2)}) async-start(), calls=%async_computation.5 | async-start | bytes 1310720 | tf_op jit(solution)/shard_map/reduce_scatter | solution.py:199
  230.4 38.0 %copy-start.21 = (f32[2048]{0:T(1024)S(1)}, f32[2048]{0:T(1024)}, u32[]{:S(2)}) copy-start(f32[2048]{0:T(1024)} %param.34) | copy-start | bytes 24580
  266.1 1.7 copy-start.7
  270.0 146.6 %copy-start.12 = (bf16[256,2048]{1,0:T(8,128)(2,1)S(1)}, bf16[256,2048]{1,0:T(8,128)(2,1)}, u32[]{:S(2)}) copy-start(bf16[256,2048]{1,0:T(8,128)(2,1)} %multiply_convert_fusion) | copy-start | bytes 3145732
  329.0 92.9 %collective-permute-start = (bf16[1,1408]{1,0:T(2,128)(2,1)S(1)}, bf16[1,1408]{1,0:T(2,128)(2,1)S(1)}, u32[]{:S(2)}, u32[]{:S(2)}) collective-permute-start(bf16[1,1408]{1,0:T(2,128)(2,1)S(1)} %get-tuple-element.436), channel_id=1, source_target_pairs={{0,4},{4,8},{8,12},{12,16},{16,20},{20,24},{24,28},{1,5},{5,9},{9,... | collective-permute-start | bytes 8456 | tf_op jit(solution)/shard_map/ppermute | solution.py:37
  331.5 90.4 %collective-permute-start.1 = (bf16[1,1408]{1,0:T(2,128)(2,1)S(1)}, bf16[1,1408]{1,0:T(2,128)(2,1)S(1)}, u32[]{:S(2)}, u32[]{:S(2)}) collective-permute-start(bf16[1,1408]{1,0:T(2,128)(2,1)S(1)} %get-tuple-element.437), channel_id=1, source_target_pairs={{4,0},{8,4},{12,8},{16,12},{20,16},{24,20},{28,24},{5,1},{9,5},{13... | collective-permute-start | bytes 8456 | tf_op jit(solution)/shard_map/ppermute | solution.py:39
  517.2 25.5 %copy-start.22 = (f32[2048]{0:T(1024)S(1)}, f32[2048]{0:T(1024)}, u32[]{:S(2)}) copy-start(f32[2048]{0:T(1024)} %param.39) | copy-start | bytes 24580
Sparse Core Ops, SparseCore 0:
  228.7 37.4 all-reduce.1
  517.4 22.9 reduce-scatter.1
Sparse Core Ops, SparseCore 1:
  231.2 93.0 all-gather.7
  326.3 90.2 all-gather.9
  418.5 91.0 all-gather.11
where the time goes:
time: 560 us; the launch traced here: 552 us
  waiting for transfers between devices  285 us (51%)
  blocking collectives  124 us (22%)
  other arithmetic  74.1 us (13%)
  matrix products  31 us (6%)
  local copies, waits for them, and re-layouts  18.2 us (3%)
  between operations  15.8 us (3%)
    all_gather x4, blocking collectives, carried_in(): pieces = jax.tree.map(lambda part: lax.all_gather(part, axis), value)  124 us
    all_gather x1, waiting for transfers between devices, shards(): lax.all_gather(w_down, 'sp', axis=1, tiled=True)  86.4 us
    all_gather x1, waiting for transfers between devices, shards(): lax.all_gather(w_value, 'sp', axis=0, tiled=True)  83.8 us
    all_gather x1, waiting for transfers between devices, shards(): lax.all_gather(w_gate, 'sp', axis=0, tiled=True)  54.2 us
    psum x1, waiting for transfers between devices, shards(): lax.psum(jnp.dot(channels, w_out, preferred_element_type=jnp.float32).ast...  35.7 us
    mul x1, other arithmetic, local_pass(): jnp.exp(-pair_re * within) * jnp.cos(pair_im * within + phase_shift)  29.3 us
    reduce_scatter x1, waiting for transfers between devices, shards(): lax.psum_scatter(partials.astype(jnp.bfloat16), 'tp', scatter_dimension=0...  23.1 us
    sub x1, other arithmetic, local_pass(): driven = complex_mul(complex_mul(decays - identity_pair, rate_inv), inflow)  14.3 us
  transfers between devices with their start and end apart: 7, of which 5 were waited for; matrix products, arithmetic and copies ran while one was open for 3% of the time, Pallas kernels for 0%

commit v1 on v0

--- a/solution.py
+++ b/solution.py
@@ -170,8 +170,11 @@
         jnp.float32
     )
     channels = jax.nn.gelu(readout).astype(jnp.bfloat16)
-    mixed = lax.psum(
-        jnp.dot(channels, w_out, preferred_element_type=jnp.float32).astype(jnp.bfloat16), "tp"
+    mixed = jnp.sum(
+        lax.all_gather(
+            jnp.dot(channels, w_out, preferred_element_type=jnp.float32).astype(jnp.bfloat16), "tp"
+        ),
+        axis=0,
     ).astype(jnp.float32)
     whole_rows = normalize(deep_alpha * residual.astype(jnp.float32) + mixed, gain_mix).astype(
         jnp.bfloat16

time: 560 us -> 593 us (1.059)
  waiting for transfers between devices: 285 us -> 318 us
    psum x1 -> x0, waiting for transfers between devices: 35.7 us -> none  [shards(): lax.psum(jnp.dot(channels, w_out, preferred_element_type=jnp.float32).ast...]
    all_gather x1, waiting for transfers between devices: 54.2 us -> 88.8 us  [shards(): lax.all_gather(w_gate, 'sp', axis=0, tiled=True)]
    all_gather x0 -> x1, waiting for transfers between devices: none -> 33.3 us  [shards(): lax.all_gather(jnp.dot(channels, w_out, preferred_element_type=jnp.float3...]
where the time goes in v1:
time: 593 us; the launch traced here: 585 us
  waiting for transfers between devices  318 us (54%)
  blocking collectives  124 us (21%)
  other arithmetic  76 us (13%)
  matrix products  31 us (5%)
  local copies, waits for them, and re-layouts  18.2 us (3%)
  between operations  13.9 us (2%)
    all_gather x4, blocking collectives, carried_in(): pieces = jax.tree.map(lambda part: lax.all_gather(part, axis), value)  124 us
    all_gather x1, waiting for transfers between devices, shards(): lax.all_gather(w_gate, 'sp', axis=0, tiled=True)  88.8 us
    all_gather x1, waiting for transfers between devices, shards(): lax.all_gather(w_down, 'sp', axis=1, tiled=True)  86.7 us
    all_gather x1, waiting for transfers between devices, shards(): lax.all_gather(w_value, 'sp', axis=0, tiled=True)  83.9 us
    all_gather x1, waiting for transfers between devices, shards(): lax.all_gather(jnp.dot(channels, w_out, preferred_element_type=jnp.float3...  33.3 us
    mul x1, other arithmetic, local_pass(): jnp.exp(-pair_re * within) * jnp.cos(pair_im * within + phase_shift)  29.3 us
    reduce_scatter x1, waiting for transfers between devices, shards(): lax.psum_scatter(partials.astype(jnp.bfloat16), 'tp', scatter_dimension=0...  23.1 us
    sub x1, other arithmetic, local_pass(): driven = complex_mul(complex_mul(decays - identity_pair, rate_inv), inflow)  14.3 us
  transfers between devices with their start and end apart: 7, of which 5 were waited for; matrix products, arithmetic and copies ran while one was open for 3% of the time, Pallas kernels for 0%

profile of v1, /device:TPU:0, one launch (start us, length us, event | category | flops | bytes accessed | tf_op | source)
XLA Modules:
  0.0 585.4 jit_solution(13357672069008758238)
XLA Ops:
  6.5 0.9 rev.15
  7.4 0.8 reduce_window_sum.21
  8.2 0.7 copy.123
  8.9 0.7 exp.21
  9.5 1.0 copy.31
  10.5 0.3 rev.16
  10.9 1.4 convolution_bitcast_fusion.1
  12.3 1.8 convolution_bitcast_fusion
  14.4 14.3 %multiply_add_fusion.12 = (f32[256,16,128]{0,2,1:T(8,128)S(1)}, f32[256,16,128]{0,2,1:T(8,128)S(1)}) fusion(f32[256]{0:T(256)S(1)} %rev.15, f32[16,128]{1,0:T(8,128)S(1)} %copy-done.22, f32[128]{0:T(128)S(1)} %copy-done.24, f32[16,128]{1,0:T(8,128)S(1)} %get-tuple-element.459, f32[16,128]{1,0:T(8,128)S(1)} %get-tuple-element.399, f32[256]{0:T(256)S(1)} %copy-done.19), kind=kLoop, calls=%fused_computation.76 | loop fusion | flops 5242880 | bytes 4221440 | tf_op jit(solution)/shard_map/sub | solution.py:83
  28.7 1.1 multiply_subtract_fusion.10
  29.8 1.6 pad_maximum_fusion.4
  31.4 1.9 copy.54
  33.3 0.2 reduce_window_sum.24
  33.8 29.3 %fusion.9 = (f32[4,64,16,128]{3,1,0,2:T(8,128)S(1)}, f32[4,64,16,128]{3,1,0,2:T(8,128)}, f32[4,64,16,128]{3,1,0,2:T(8,128)S(1)}, f32[4,64,16,128]{3,1,0,2:T(8,128)S(1)}) fusion(f32[4,64]{1,0:T(4,128)S(1)} %reduce_window_sum.24, f32[128]{0:T(128)S(1)} %copy-done.26, f32[16,128]{1,0:T(8,128)S(1)} %get-tuple-element.398, f32[16,128]{1,0:T(8,128)S(1)} %get-tuple-element.459, ...), kind=kLoop, calls=%fused_computation.48 | loop fusion | flops 7340032 | bytes 8416256 | tf_op jit(solution)/shard_map/mul | solution.py:86
  63.1 1.6 multiply_subtract_fusion.7
  64.8 1.6 fusion.10
  66.4 0.4 copy.64
  66.8 1.0 copy-done.4
  67.9 0.8 while.61
  68.7 32.3 %all-gather.2 = f32[128,128]{1,0:T(8,128)S(1)} all-gather(f32[16,128]{1,0:T(8,128)S(1)} %get-tuple-element.280), channel_id=4, replica_groups=mesh['sp'=8,'tp'=4] {'sp'}, dimensions={0}, use_global_device_ids=true | all-gather | bytes 73728 | tf_op jit(solution)/shard_map/all_gather | solution.py:14
  101.0 30.5 %all-gather.3 = f32[128,128]{1,0:T(8,128)S(1)} all-gather(f32[16,128]{1,0:T(8,128)S(1)} %get-tuple-element.281), channel_id=5, replica_groups=mesh['sp'=8,'tp'=4] {'sp'}, dimensions={0}, use_global_device_ids=true | all-gather | bytes 73728 | tf_op jit(solution)/shard_map/all_gather | solution.py:14
  131.6 1.4 while.63
  133.1 0.8 maximum_add_fusion.3
  134.0 2.0 bitcast_add_fusion.2
  136.2 1.6 multiply_subtract_fusion.6
  137.8 2.7 fusion.36
  140.4 1.0 copy.48
  141.5 2.1 reshape.197
  143.5 1.8 rev.19
  145.3 3.0 copy.52
  148.3 4.6 multiply_subtract_fusion.9
  152.9 1.6 fusion.13
  154.5 0.4 copy.63
  154.9 1.0 copy-done.5
  155.9 0.8 while.60
  156.7 30.5 %all-gather = f32[128,128]{1,0:T(8,128)S(1)} all-gather(f32[16,128]{1,0:T(8,128)S(1)} %get-tuple-element.275), channel_id=2, replica_groups=mesh['sp'=8,'tp'=4] {'sp'}, dimensions={0}, use_global_device_ids=true | all-gather | bytes 73728 | tf_op jit(solution)/shard_map/all_gather | solution.py:14
  187.2 30.5 %all-gather.1 = f32[128,128]{1,0:T(8,128)S(1)} all-gather(f32[16,128]{1,0:T(8,128)S(1)} %get-tuple-element.276), channel_id=3, replica_groups=mesh['sp'=8,'tp'=4] {'sp'}, dimensions={0}, use_global_device_ids=true | all-gather | bytes 73728 | tf_op jit(solution)/shard_map/all_gather | solution.py:14
  217.8 1.4 while.62
  219.5 1.9 bitcast_add_fusion.3
  221.4 1.3 multiply_subtract_fusion.8
  222.7 2.7 fusion.39
  225.6 0.3 reshape.193
  226.3 1.5 convolution_convert_fusion.2
  227.8 0.7 all-gather.10.cloned.1.call-update
  228.5 0.7 all-gather.12.cloned.1.call-update
  229.3 0.5 all-gather.14.cloned.1.call-update
  229.9 33.3 %all-gather.16.cloned.1.call-done = bf16[1024,2048]{1,0:T(8,128)(2,1)} async-done(((bf16[256,2048]{1,0:T(8,128)(2,1)}), bf16[1024,2048]{1,0:T(8,128)(2,1)}) %all-gather.16.cloned.1.call-update) | async-done | bytes 4194320 | tf_op jit(solution)/shard_map/all_gather | solution.py:174
  263.2 3.2 reduce_sum.48
  266.4 0.4 fusion.24
  266.8 0.6 multiply_reduce_fusion
  267.4 1.6 multiply_convert_fusion
  269.0 88.8 %all-gather.10.cloned.1.call-done = bf16[2048,1408]{1,0:T(8,128)(2,1)} async-done(((bf16[256,1408]{1,0:T(8,128)(2,1)}), bf16[2048,1408]{1,0:T(8,128)(2,1)}) %all-gather.10.cloned.1.call-update) | async-done | bytes 5767184 | tf_op jit(solution)/shard_map/all_gather | solution.py:186
  357.8 4.8 convolution_convert_fusion.1
  362.5 2.5 collective-permute-start
  365.0 1.5 collective-permute-start.1
  366.6 83.9 %all-gather.12.cloned.1.call-done = bf16[2048,1408]{1,0:T(8,128)(2,1)} async-done(((bf16[256,1408]{1,0:T(8,128)(2,1)}), bf16[2048,1408]{1,0:T(8,128)(2,1)}) %all-gather.12.cloned.1.call-update) | async-done | bytes 5767184 | tf_op jit(solution)/shard_map/all_gather | solution.py:191
  450.5 5.3 convolution_convert_fusion
  455.8 1.3 maximum_convert_fusion
  457.1 86.7 %all-gather.14.cloned.1.call-done = bf16[1408,2048]{1,0:T(8,128)(2,1)} async-done(((bf16[1408,256]{1,0:T(8,128)(2,1)}), bf16[1408,2048]{1,0:T(8,128)(2,1)}) %all-gather.14.cloned.1.call-update) | async-done | bytes 5767184 | tf_op jit(solution)/shard_map/all_gather | solution.py:200
  543.7 7.7 %convolution_convert_fusion.3 = bf16[256,2048]{1,0:T(8,128)(2,1)} fusion(bf16[1408,2048]{1,0:T(8,128)(2,1)} %all-gather.14.cloned.1.call-done, f32[258,1408]{1,0:T(8,128)} %maximum_convert_fusion, bf16[256,1408]{1,0:T(8,128)(2,1)} %convolution_convert_fusion, f32[1408]{0:T(1024)S(1)} %get-tuple-element.348, f32[1408]{0:T(1024)S(1)} %get-tuple-element.349, ...), kind=kOutput, calls=%fused_computation.39 | convolution fusion | flops 1482686464 | bytes 11878912 | tf_op jit(solution)/shard_map/dot_general | solution.py:199
  551.4 23.1 %reduce-scatter.2.cloned.1.call-done = bf16[64,2048]{1,0:T(8,128)(2,1)} async-done(((bf16[256,2048]{1,0:T(8,128)(2,1)}), bf16[64,2048]{1,0:T(8,128)(2,1)}) %reduce-scatter.2.cloned.1.call-update) | async-done | bytes 262160 | tf_op jit(solution)/shard_map/reduce_scatter | solution.py:202
  574.5 1.1 fusion.50
  575.7 1.2 multiply_reduce_fusion.1
  576.9 1.8 multiply_convert_fusion.1
  (192 shorter events, 5.7 us)
Async XLA Ops:
  6.5 219.7 %copy-start = (bf16[256,2048]{1,0:T(8,128)(2,1)S(1)}, bf16[256,2048]{1,0:T(8,128)(2,1)}, u32[]{:S(2)}) copy-start(bf16[256,2048]{1,0:T(8,128)(2,1)} %param.33) | copy-start | bytes 3145732
  6.5 256.7 %all-gather.16.cloned.1.call-start = ((), (), s32[]{:S(2)}) async-start(), calls=%async_computation.5 | async-start | bytes 5242880 | tf_op jit(solution)/shard_map/all_gather | solution.py:174
  8.9 5.3 copy-start.8
  10.8 1.5 copy-start.15
  10.8 3.4 copy-start.17
  10.8 3.4 copy-start.23
  10.8 3.5 copy-start.19
  10.9 3.5 copy-start.22
  10.9 3.5 copy-start.24
  14.3 14.3 %copy-start.7 = (f32[256,16,128]{0,2,1:T(8,128)S(1)}, f32[256,16,128]{0,2,1:T(8,128)}, u32[]{:S(2)}) copy-start(f32[256,16,128]{0,2,1:T(8,128)} %convolution_bitcast_fusion) | copy-start | bytes 6291460
  31.4 2.4 copy-start.26
  33.8 29.3 %copy-start.3 = (f32[256,16,128]{2,0,1:T(8,128)S(1)}, f32[256,16,128]{2,0,1:T(8,128)}, u32[]{:S(2)}) copy-start(f32[256,16,128]{2,0,1:T(8,128)} %copy.54) | copy-start | bytes 6291460
  63.1 4.7 copy-start.1
  66.4 1.4 copy-start.4
  66.4 1.5 copy-start.10
  68.7 32.3 %copy-start.16 = (f32[4,16,128]{2,1,0:T(8,128)}, f32[4,16,128]{2,1,0:T(8,128)S(1)}, u32[]{:S(2)}) copy-start(f32[4,16,128]{2,1,0:T(8,128)S(1)} %get-tuple-element.278) | copy-start | bytes 98308
  134.0 2.2 copy-start.2
  136.2 1.6 copy-start.13
  154.5 1.4 copy-start.5
  154.5 1.4 copy-start.9
  221.4 1.3 copy-start.14
  222.7 3.2 copy-start.12
  225.4 0.7 copy-start.25
  227.7 2.1 copy-start.18
  227.7 130.0 %all-gather.10.cloned.1.call-start = ((), (), s32[]{:S(2)}) async-start(), calls=%async_computation.1 | async-start | bytes 6488064 | tf_op jit(solution)/shard_map/all_gather | solution.py:186
  228.5 222.0 %all-gather.12.cloned.1.call-start = ((), (), s32[]{:S(2)}) async-start(), calls=%async_computation.2 | async-start | bytes 6488064 | tf_op jit(solution)/shard_map/all_gather | solution.py:191
  229.2 314.5 %all-gather.14.cloned.1.call-start = ((), (), s32[]{:S(2)}) async-start(), calls=%async_computation.3 | async-start | bytes 6488064 | tf_op jit(solution)/shard_map/all_gather | solution.py:200
  229.8 344.7 %reduce-scatter.2.cloned.1.call-start = ((), (), s32[]{:S(2)}) async-start(), calls=%async_computation.4 | async-start | bytes 1310720 | tf_op jit(solution)/shard_map/reduce_scatter | solution.py:202
  263.2 3.2 copy-start.6
  266.4 1.0 copy-start.20
  269.0 181.5 %copy-start.11 = (bf16[256,2048]{1,0:T(8,128)(2,1)S(1)}, bf16[256,2048]{1,0:T(8,128)(2,1)}, u32[]{:S(2)}) copy-start(bf16[256,2048]{1,0:T(8,128)(2,1)} %multiply_convert_fusion) | copy-start | bytes 3145732
  362.5 93.2 %collective-permute-start = (bf16[1,1408]{1,0:T(2,128)(2,1)S(1)}, bf16[1,1408]{1,0:T(2,128)(2,1)S(1)}, u32[]{:S(2)}, u32[]{:S(2)}) collective-permute-start(bf16[1,1408]{1,0:T(2,128)(2,1)S(1)} %get-tuple-element.436), channel_id=1, source_target_pairs={{0,4},{4,8},{8,12},{12,16},{16,20},{20,24},{24,28},{1,5},{5,9},{9,... | collective-permute-start | bytes 8456 | tf_op jit(solution)/shard_map/ppermute | solution.py:37
  365.0 90.8 %collective-permute-start.1 = (bf16[1,1408]{1,0:T(2,128)(2,1)S(1)}, bf16[1,1408]{1,0:T(2,128)(2,1)S(1)}, u32[]{:S(2)}, u32[]{:S(2)}) collective-permute-start(bf16[1,1408]{1,0:T(2,128)(2,1)S(1)} %get-tuple-element.437), channel_id=1, source_target_pairs={{4,0},{8,4},{12,8},{16,12},{20,16},{24,20},{28,24},{5,1},{9,5},{13... | collective-permute-start | bytes 8456 | tf_op jit(solution)/shard_map/ppermute | solution.py:39
  551.4 25.5 %copy-start.21 = (f32[2048]{0:T(1024)S(1)}, f32[2048]{0:T(1024)}, u32[]{:S(2)}) copy-start(f32[2048]{0:T(1024)} %param.39) | copy-start | bytes 24580
Sparse Core Ops, SparseCore 0:
  227.9 35.3 all-gather.15
  265.4 92.3 all-gather.9
  359.9 90.4 all-gather.11
  452.4 91.3 all-gather.13
  551.5 22.9 reduce-scatter.1
